TPU v7x, 512 devices: a whole 4x8x8 slice. The times are simulated.
512 devices in a mesh: sp: 64 (over z, y), tp: 8 (over x, core).
Axes of the slice: x: 4, y: 8, z: 8, core: 2. Of those that a mesh axis runs over, the one named last changes fastest.
Arguments:
- tokens: bfloat16 [16384, 2048], P(('sp', 'tp')), may hold values from -6 to 6
- norm_gain: float32 [2048], replicated, may hold values from 0.1 to 1.9
- w_query: bfloat16 [2048, 1024], P('sp', 'tp'), may hold values from -0.125 to 0.125
- w_forget: bfloat16 [2048, 1024], P('sp', 'tp'), may hold values from -0.125 to 0.125
- w_value: bfloat16 [2048, 1024], P('sp', 'tp'), may hold values from -0.125 to 0.125
- w_outgate: bfloat16 [2048, 1024], P('sp', 'tp'), may hold values from -0.125 to 0.125
- leak: float32 [1024], P('tp'), may hold values from 1.2207031e-05 to 6.1035156e-05
- decay_shift: float32 [16384, 1024], P('sp', 'tp'), may hold values from -1 to 0
- head_gain: float32 [128], replicated, may hold values from 0.1 to 1.9
- w_glu_value: bfloat16 [2048, 2048], P('sp', 'tp'), may hold values from -0.125 to 0.125
- w_glu_gate: bfloat16 [2048, 2048], P('sp', 'tp'), may hold values from -0.125 to 0.125
- conv_kernel: float32 [31, 2048], P(None, 'tp'), may hold values from -20 to 20
- ln_gain: float32 [2048], P('tp'), may hold values from 0.1 to 1.9
- ln_bias: float32 [2048], P('tp'), may hold values from -3 to 3
- w_out_rec: bfloat16 [1024, 2048], P('tp', 'sp'), may hold values from -0.125 to 0.125
- w_out_conv: bfloat16 [2048, 2048], P('tp', 'sp'), may hold values from -0.09375 to 0.09375
Outputs:
- mixed: bfloat16 [16384, 2048], P(('sp', 'tp'))
All inputs are finite; a program needn't handle non-finite values.
Results may differ from a plain program's by a relative error of at most 0.019.
Values may be sent and summed in bfloat16 or wider, within the bound.
No kernel may reach another device: no remote copies, remote signals or barrier semaphores. Data moves between devices by JAX's collectives and lax.ppermute only.
A program may use at most 64 MiB of HBM per device.

v0:
```python
import jax
import jax.numpy as jnp
from jax import lax
from jax.sharding import Mesh
from jax.sharding import PartitionSpec as P

HEAD_K = 128
HEAD_V = 128
KERNEL = 31
BLOCK = 64
SP = ("sp_0", "sp_1")
SP_TP = ("sp_0", "sp_1", "tp")


def turned_gather(arrays, axis, dims):
    turned = [jnp.moveaxis(a, dim, 0) for a, dim in zip(arrays, dims)]
    widths = [t[0].size for t in turned]
    both = jnp.concatenate([t.reshape(-1, w) for t, w in zip(turned, widths)], axis=1)
    filled = lax.all_gather(both, axis, axis=0, tiled=True)
    pieces = jnp.split(filled, [sum(widths[:k]) for k in range(1, len(widths))], axis=1)
    return tuple(
        (
            jnp.moveaxis(b.reshape(-1, *t.shape[1:]), 0, dim)
            for b, t, dim in zip(pieces, turned, dims)
        )
    )


def from_everyone(value, axis):
    copies = jnp.broadcast_to(value, (lax.axis_size(axis), *value.shape))
    return lax.all_to_all(copies, axis, split_axis=0, concat_axis=0, tiled=True)


def laid_out(pieces, dim):
    lengths = list(pieces.shape[1:])
    lengths[dim] *= pieces.shape[0]
    return jnp.moveaxis(pieces, 0, dim).reshape(lengths)


def gather_directly(value, axis, dim):
    pieces = from_everyone(value, axis)
    return laid_out(pieces, dim)


def neutral_like(value, identity):
    return jax.tree.map(
        lambda a, e: jnp.broadcast_to(jnp.asarray(e, a.dtype), a.shape), value, identity
    )


def collected_together(value, axis):
    leaves = jax.tree.leaves(value)
    order = sorted(range(len(leaves)), key=lambda k: -leaves[k].size)
    width = (1, *leaves[order[0]].shape)[-1]
    lines = [
        jnp.pad(leaves[k].reshape(-1), (0, -leaves[k].size % width)).reshape(-1, width)
        for k in order
    ]
    both, at, found = (lax.all_gather(jnp.concatenate(lines), axis), 0, {})
    for k, line in zip(order, lines):
        piece = both[:, at : at + len(line)].reshape(len(both), -1)
        found[k] = piece[:, : leaves[k].size].reshape(-1, *leaves[k].shape)
        at += len(line)
    numbers = iter(range(len(leaves)))
    return jax.tree.map(lambda _: found[next(numbers)], value)


def entering(value, axes, combine, identity):
    before = start = neutral_like(value, identity)
    subtotal = value
    for axis in reversed(axes):
        peers, position = (lax.axis_size(axis), lax.axis_index(axis))
        pieces = collected_together(
            jax.tree.map(
                lambda part, kind: part.astype(kind), subtotal, (jnp.bfloat16, jnp.bfloat16)
            ),
            axis,
        )
        inside, subtotal = (start, start)
        for k in range(peers):
            passed = k < position
            subtotal = combine(
                subtotal, jax.tree.map(lambda part, own: part[k].astype(own.dtype), pieces, value)
            )
            inside = jax.tree.map(lambda new, old: jnp.where(passed, new, old), subtotal, inside)
        before = combine(inside, before)
    return before


def from_behind(value, axis, steps):
    count = lax.axis_size(axis)
    initial, last = (max(0, -steps), min(count, count - steps))
    return lax.ppermute(value, axis, [(source, source + steps) for source in range(initial, last)])


def over_copies(value, axis):
    return from_everyone(value, axis).sum(axis=0)


def in_one(arrays, axis):
    ravelled, at, done = (jnp.concatenate([a.reshape(-1) for a in arrays]), 0, [])
    subtotal = over_copies(ravelled, axis)
    for a in arrays:
        done.append(subtotal[at : at + a.size].reshape(a.shape))
        at += a.size
    return tuple(done)


def split_up(value, dim, peers):
    before, after = (value.shape[:dim], value.shape[dim + 1 :])
    return jnp.moveaxis(value.reshape(*before, peers, -1, *after), dim, 0)


def sent_and_summed(value, axis, dim):
    pieces = split_up(value, dim, lax.axis_size(axis))
    arrived = lax.all_to_all(pieces, axis, split_axis=0, concat_axis=0, tiled=True)
    return arrived.astype(jnp.float32).sum(axis=0)


def normalize(row_block, norm_gain):
    values_in = row_block.astype(jnp.float32)
    row_scale = lax.rsqrt(jnp.mean(values_in * values_in, axis=1, keepdims=True) + 1e-06)
    return (values_in * row_scale * norm_gain).astype(jnp.bfloat16)


def combine_states(earlier, later):
    return (earlier[0] + later[0], jnp.exp(later[0])[..., None] * earlier[1] + later[1])


def local_recurrence(queries, in_gate, payload_matrix_lines, log_decay):
    row_count, head_count, key_width = queries.shape
    value_width = payload_matrix_lines.shape[2]
    block_count = row_count // BLOCK

    def split_blocks(tensor):
        return tensor.reshape(block_count, BLOCK, head_count, tensor.shape[-1])

    q_blocks = split_blocks(queries)
    k_blocks = split_blocks(in_gate)
    v_blocks = split_blocks(payload_matrix_lines)
    cumulative_sum = jnp.cumsum(split_blocks(log_decay), axis=1)
    causal = jnp.tril(jnp.ones((BLOCK, BLOCK), jnp.float32))
    scores = jnp.einsum(
        "nthk,nshk->nhts", q_blocks * jnp.exp(cumulative_sum), k_blocks * jnp.exp(-cumulative_sum)
    )
    within = jnp.einsum("nhts,nshv->nthv", scores * causal, v_blocks)
    block_finish = cumulative_sum[:, -1]
    contrib = jnp.einsum(
        "nshk,nshv->nhkv", k_blocks * jnp.exp(block_finish[:, None] - cumulative_sum), v_blocks
    )

    def advance(carried_in, inputs):
        state_list, before = carried_in
        query_block, column_block, e_block, added_terms = inputs
        carried_state = jnp.einsum("aub,ubd->aud", query_block * jnp.exp(column_block), state_list)
        device_query = query_block * jnp.exp(column_block + before[None])
        state_list = jnp.exp(e_block)[..., None] * state_list + added_terms
        return ((state_list, before + e_block), (carried_state, device_query))

    initial = (
        jnp.zeros((head_count, key_width, value_width), jnp.float32),
        jnp.zeros((head_count, key_width), jnp.float32),
    )
    (state_list, totals), (carried_state, device_query) = lax.scan(
        advance, initial, (q_blocks, cumulative_sum, block_finish, contrib)
    )
    recurrence_step = (within + carried_state).reshape(row_count, head_count, value_width)
    return (
        recurrence_step,
        device_query.reshape(row_count, head_count, key_width),
        state_list,
        totals,
    )


def on_device(
    tokens,
    norm_gain,
    w_query,
    w_forget,
    w_value,
    w_outgate,
    leak,
    decay_shift,
    head_gain,
    w_glu_value,
    w_glu_gate,
    conv_kernel,
    ln_gain,
    ln_bias,
    w_out_rec,
    w_out_conv,
):
    widths = [
        w_query.shape[1],
        w_forget.shape[1],
        w_value.shape[1],
        w_outgate.shape[1],
        w_glu_value.shape[1],
        w_glu_gate.shape[1],
    ]
    gathered = turned_gather(
        (w_query, w_forget, w_value, w_outgate, w_glu_value, w_glu_gate, w_out_rec, w_out_conv),
        SP,
        (0, 0, 0, 0, 0, 0, 1, 1),
    )
    full_in = gathered[:6]
    out_rec = gathered[6]
    out_conv = gathered[7]
    normed = normalize(gather_directly(tokens, "tp", 0), norm_gain)
    joined = jnp.concatenate(
        [
            jnp.dot(normed, weight, preferred_element_type=jnp.float32).astype(jnp.bfloat16)
            for weight in full_in
        ],
        axis=1,
    )
    projections = []
    column = 0
    for width_now in widths:
        projections.append(joined[:, column : column + width_now])
        column = column + width_now
    query_pre, forget_pre, value_pre, gate_pre, glu_value_pre, glu_gate_pre = projections
    row_count = query_pre.shape[0]
    head_count = query_pre.shape[1] // HEAD_K
    queries = jax.nn.silu(query_pre.astype(jnp.float32))
    in_gate = leak * jax.nn.sigmoid(-forget_pre.astype(jnp.float32))
    log_decay = jnp.log1p(-in_gate) + decay_shift
    recurrence_step, device_query, state_list, totals = local_recurrence(
        queries.reshape(row_count, head_count, HEAD_K),
        in_gate.reshape(row_count, head_count, HEAD_K),
        value_pre.astype(jnp.float32).reshape(row_count, head_count, HEAD_V),
        log_decay.reshape(row_count, head_count, HEAD_K),
    )
    _, incoming_state = entering(
        (totals, state_list),
        SP,
        combine_states,
        (jnp.zeros_like(totals), jnp.zeros_like(state_list)),
    )
    recurrence_step = recurrence_step + jnp.einsum("aub,ubd->aud", device_query, incoming_state)
    scaling = lax.rsqrt(jnp.mean(recurrence_step * recurrence_step, axis=2, keepdims=True) + 1e-06)
    gate_act = jax.nn.silu(gate_pre.astype(jnp.float32)).reshape(row_count, head_count, HEAD_V)
    head_out = (
        (recurrence_step * scaling * head_gain * gate_act)
        .reshape(row_count, head_count * HEAD_V)
        .astype(jnp.bfloat16)
    )
    glu = (
        glu_value_pre.astype(jnp.float32) * jax.nn.sigmoid(glu_gate_pre.astype(jnp.float32))
    ).astype(jnp.bfloat16)
    left_rim = from_behind(glu[row_count - (KERNEL - 1) :], SP, 1)
    extended = jnp.concatenate([left_rim, glu], axis=0).astype(jnp.float32)

    def add_tap(tap_index, accum):
        taps = lax.dynamic_slice_in_dim(conv_kernel, tap_index, 1, 0)
        return accum + taps * lax.dynamic_slice_in_dim(extended, tap_index, row_count, 0)

    conv_sum = lax.fori_loop(0, KERNEL, add_tap, jnp.zeros((row_count, glu.shape[1]), jnp.float32))
    channel_count = conv_sum.shape[1] * lax.axis_size("tp")
    sum_rows, square_rows = in_one(
        (
            jnp.sum(conv_sum, axis=1, keepdims=True),
            jnp.sum(conv_sum * conv_sum, axis=1, keepdims=True),
        ),
        "tp",
    )
    row_mean = sum_rows / channel_count
    centered = conv_sum - row_mean
    row_var = square_rows / channel_count - row_mean * row_mean
    conv_out = jax.nn.silu(centered * lax.rsqrt(row_var + 1e-05) * ln_gain + ln_bias).astype(
        jnp.bfloat16
    )
    mixed = sent_and_summed(
        (
            jnp.dot(head_out, out_rec, preferred_element_type=jnp.float32)
            + jnp.dot(conv_out, out_conv, preferred_element_type=jnp.float32)
        ).astype(jnp.bfloat16),
        "tp",
        0,
    )
    return mixed.astype(jnp.bfloat16)


def solution(mesh):
    torus = Mesh(mesh.devices.reshape(8, 8, mesh.shape["tp"]), ("sp_0", "sp_1", "tp"))
    placed = (
        P(SP_TP, None),
        P(),
        P(SP, "tp"),
        P(SP, "tp"),
        P(SP, "tp"),
        P(SP, "tp"),
        P("tp"),
        P(SP, "tp"),
        P(),
        P(SP, "tp"),
        P(SP, "tp"),
        P(None, "tp"),
        P("tp"),
        P("tp"),
        P("tp", SP),
        P("tp", SP),
    )
    return jax.shard_map(
        on_device, mesh=torus, in_specs=placed, out_specs=P(SP_TP, None), check_vma=False
    )
```

profile of v0, /device:TPU:64, one launch (start us, length us, event | category | flops | bytes accessed | tf_op | source)
XLA Modules:
  0.0 237.1 jit_solution(12225472231829536616)
XLA Ops:
  6.5 0.7 constant_dynamic-update-slice_fusion.7
  9.4 0.7 constant_dynamic-update-slice_fusion.3
  12.9 2.0 broadcast_in_dim.19
  14.9 4.3 %all-to-all-start = ((bf16[8,32,2048]{2,1,0:T(8,128)(2,1)}), bf16[8,32,2048]{2,1,0:T(8,128)(2,1)S(1)}, u32[]{:S(2)}, u32[]{:S(2)}) async-start(bf16[8,32,2048]{2,1,0:T(8,128)(2,1)} %broadcast_in_dim.19), calls=%async_computation | async-start | bytes 2097152 | tf_op jit(solution)/shard_map/all_to_all | solution.py:31
  19.3 15.8 %all-to-all-done = bf16[8,32,2048]{2,1,0:T(8,128)(2,1)S(1)} async-done(((bf16[8,32,2048]{2,1,0:T(8,128)(2,1)}), bf16[8,32,2048]{2,1,0:T(8,128)(2,1)S(1)}, u32[]{:S(2)}, u32[]{:S(2)}) %all-to-all-start) | async-done | bytes 1048608 | tf_op jit(solution)/shard_map/all_to_all | solution.py:31
  35.5 1.0 fusion.9
  36.6 69.1 %all-gather.6.cloned.1.call-done = bf16[2048,1408]{1,0:T(8,128)(2,1)} async-done(((bf16[32,1408]{1,0:T(8,128)(2,1)}), bf16[2048,1408]{1,0:T(8,128)(2,1)}) %all-gather.6.cloned.1.call-update) | async-done | bytes 5767184 | tf_op jit(solution)/shard_map/all_gather | solution.py:19
  105.7 1.5 log-plus-one_add_fusion
  107.3 1.5 convolution_convert_fusion.5
  109.0 1.5 divide_multiply_fusion
  110.5 1.5 while.31
  112.1 25.0 %all-gather.2 = bf16[8,129,128]{2,1,0:T(8,128)(2,1)S(1)} all-gather(bf16[1,129,128]{2,1,0:T(8,128)(2,1)S(1)} %maximum_bitcast_fusion), channel_id=2, replica_groups=mesh['sp_0'=8,'sp_1'=8,'tp'=8] {'sp_1'}, dimensions={0}, use_global_device_ids=true | all-gather | bytes 297216 | tf_op jit(solution)/shard_map/all_gather | solution.py:59
  137.3 24.6 %all-gather.3 = bf16[8,129,128]{2,1,0:T(8,128)(2,1)S(1)} all-gather(bf16[1,129,128]{2,1,0:T(8,128)(2,1)S(1)} %maximum_bitcast_fusion.1), channel_id=3, replica_groups=mesh['sp_0'=8,'sp_1'=8,'tp'=8] {'sp_0'}, dimensions={0}, use_global_device_ids=true | all-gather | bytes 297216 | tf_op jit(solution)/shard_map/all_gather | solution.py:59
  162.0 1.7 fusion.17
  163.6 1.7 fusion.16
  165.3 2.7 %collective-permute-start = (bf16[30,256]{1,0:T(8,128)(2,1)S(1)}, bf16[30,256]{1,0:T(8,128)(2,1)S(1)}, u32[]{:S(2)}, u32[]{:S(2)}) collective-permute-start(bf16[30,256]{1,0:T(8,128)(2,1)S(1)} %slice.229), channel_id=1, source_target_pairs={{0,8},{8,16},{16,24},{24,32},{32,40},{40,48},{48,56},{56,64},{64,7... | collective-permute-start | bytes 46088 | tf_op jit(solution)/shard_map/ppermute | solution.py:93
  169.6 3.5 %collective-permute-done = bf16[30,256]{1,0:T(8,128)(2,1)S(1)} collective-permute-done((bf16[30,256]{1,0:T(8,128)(2,1)S(1)}, bf16[30,256]{1,0:T(8,128)(2,1)S(1)}, u32[]{:S(2)}, u32[]{:S(2)}) %collective-permute-start) | collective-permute-done | bytes 15392 | tf_op jit(solution)/shard_map/ppermute | solution.py:93
  173.1 25.7 %while.32 = (s32[]{:T(128)}, f32[256,256]{1,0:T(8,128)S(1)}, f32[31,256]{1,0:T(8,128)}, f32[286,256]{1,0:T(8,128)S(1)}, s32[]{:T(128)}, /*index=5*/s32[]{:T(128)}) while((s32[]{:T(128)}, f32[256,256]{1,0:T(8,128)S(1)}, f32[31,256]{1,0:T(8,128)}, f32[286,256]{1,0:T(8,128)S(1)}, s32[]{:T(128)}, /*index=5*/s32[]{:T(128)}) %tuple.82), condition=%wide.region_6.7_spmd.clone, body=%wide.region_5.6_spmd.clone.sunk | while | flops 196611 | bytes 789591 | solution.py:259
  199.6 4.3 %all-to-all-start.1 = ((f32[8,1,512]{2,1,0:T(1,128)}), f32[8,1,512]{2,1,0:T(1,128)S(1)}, u32[]{:S(2)}, u32[]{:S(2)}) async-start(f32[8,1,512]{2,1,0:T(1,128)} %broadcast_in_dim.23), calls=%async_computation.1 | async-start | bytes 32768 | tf_op jit(solution)/shard_map/all_to_all | solution.py:31
  203.9 2.0 fusion.30
  205.9 3.3 %all-to-all-done.1 = f32[8,1,512]{2,1,0:T(1,128)S(1)} async-done(((f32[8,1,512]{2,1,0:T(1,128)}), f32[8,1,512]{2,1,0:T(1,128)S(1)}, u32[]{:S(2)}, u32[]{:S(2)}) %all-to-all-start.1) | async-done | bytes 16416 | tf_op jit(solution)/shard_map/all_to_all | solution.py:31
  209.3 1.8 fusion.7
  211.1 18.4 %all_to_all.16 = bf16[8,32,2048]{2,1,0:T(8,128)(2,1)S(1)} all-to-all(bf16[8,32,2048]{2,1,0:T(8,128)(2,1)S(1)} %bitcast.158), channel_id=1, replica_groups=mesh['sp_0'=8,'sp_1'=8,'tp'=8] {'tp'}, dimensions={0} | all-to-all | bytes 2097152 | tf_op jit(solution)/shard_map/all_to_all | solution.py:116
  229.4 0.8 reduce_sum.62
  (126 shorter events, 34.8 us)
Async XLA Ops:
  6.5 99.2 %copy-start.2 = (f32[128]{0:T(128)S(1)}, f32[128]{0:T(128)}, u32[]{:S(2)}) copy-start(f32[128]{0:T(128)} %param.26) | copy-start | bytes 1540
  6.5 99.2 %copy-start.1 = (f32[256,128]{1,0:T(8,128)S(1)}, f32[256,128]{1,0:T(8,128)}, u32[]{:S(2)}) copy-start(f32[256,128]{1,0:T(8,128)} %param.27) | copy-start | bytes 393220
  6.5 99.2 %all-gather.6.cloned.1.call-start = ((), (), s32[]{:S(2)}) async-start(), calls=%async_computation.3 | async-start | bytes 5857280 | tf_op jit(solution)/shard_map/all_gather | solution.py:19
  12.3 0.6 copy-start
  14.9 20.2 %all-to-all-start = ((bf16[8,32,2048]{2,1,0:T(8,128)(2,1)}), bf16[8,32,2048]{2,1,0:T(8,128)(2,1)S(1)}, u32[]{:S(2)}, u32[]{:S(2)}) async-start(bf16[8,32,2048]{2,1,0:T(8,128)(2,1)} %broadcast_in_dim.19), calls=%async_computation | async-start | bytes 2097152 | tf_op jit(solution)/shard_map/all_to_all | solution.py:31
  165.3 7.7 %collective-permute-start = (bf16[30,256]{1,0:T(8,128)(2,1)S(1)}, bf16[30,256]{1,0:T(8,128)(2,1)S(1)}, u32[]{:S(2)}, u32[]{:S(2)}) collective-permute-start(bf16[30,256]{1,0:T(8,128)(2,1)S(1)} %slice.229), channel_id=1, source_target_pairs={{0,8},{8,16},{16,24},{24,32},{32,40},{40,48},{48,56},{56,64},{64,7... | collective-permute-start | bytes 46088 | tf_op jit(solution)/shard_map/ppermute | solution.py:93
  199.6 9.6 %all-to-all-start.1 = ((f32[8,1,512]{2,1,0:T(1,128)}), f32[8,1,512]{2,1,0:T(1,128)S(1)}, u32[]{:S(2)}, u32[]{:S(2)}) async-start(f32[8,1,512]{2,1,0:T(1,128)} %broadcast_in_dim.23), calls=%async_computation.1 | async-start | bytes 32768 | tf_op jit(solution)/shard_map/all_to_all | solution.py:31
Sparse Core Ops, SparseCore 0:
  13.0 92.6 all-gather.5
where the time goes:
time: 240 us; the launch traced here: 237 us
  waiting for transfers between devices  91.9 us (38%)
  blocking collectives  68 us (28%)
  local copies, waits for them, and re-layouts  31 us (13%)
  between operations  13.7 us (6%)
  matrix products  13.2 us (6%)
  starting transfers between devices  11.2 us (5%)
  other arithmetic  7.44 us (3%)
    all_gather x1, waiting for transfers between devices, turned_gather(): filled = lax.all_gather(both, axis, axis=0, tiled=True)  69.1 us
    all_gather x2, blocking collectives, collected_together(): both, at, found = (lax.all_gather(jnp.concatenate(lines), axis), 0, {})  49.6 us
    dynamic_slice x31, local copies, waits for them, and re-layouts, add_tap(): taps = lax.dynamic_slice_in_dim(conv_kernel, tap_index, 1, 0)  21.9 us
    all_to_all x2, waiting for transfers between devices, from_everyone(): return lax.all_to_all(copies, axis, split_axis=0, concat_axis=0, tiled=True)  19.2 us
    all_to_all x1, blocking collectives, sent_and_summed(): lax.all_to_all(pieces, axis, split_axis=0, concat_axis=0, tiled=True)  18.4 us
    all_to_all x2, starting transfers between devices, from_everyone(): return lax.all_to_all(copies, axis, split_axis=0, concat_axis=0, tiled=True)  8.55 us
    dot_general x5, matrix products, on_device(): jnp.dot(normed, weight, preferred_element_type=jnp.float32)  7.78 us
    unnamed x14, local copies, waits for them, and re-layouts  5.64 us
  transfers between devices with their start and end apart: 4, of which 4 were waited for; matrix products, arithmetic and copies ran while one was open for 3% of the time, Pallas kernels for 0%

commit v1 on v0

--- a/solution.py
+++ b/solution.py
@@ -12,11 +12,18 @@
 SP_TP = ("sp_0", "sp_1", "tp")
 
 
+def swapped_in(x, name, along):
+    size = lax.axis_size(name)
+    shards = jnp.stack([x for _ in range(size)])
+    shards = lax.all_to_all(shards, name, split_axis=0, concat_axis=0)
+    return jnp.concatenate(shards, axis=along)
+
+
 def turned_gather(arrays, axis, dims):
     turned = [jnp.moveaxis(a, dim, 0) for a, dim in zip(arrays, dims)]
     widths = [t[0].size for t in turned]
     both = jnp.concatenate([t.reshape(-1, w) for t, w in zip(turned, widths)], axis=1)
-    filled = lax.all_gather(both, axis, axis=0, tiled=True)
+    filled = swapped_in(both, axis, 0)
     pieces = jnp.split(filled, [sum(widths[:k]) for k in range(1, len(widths))], axis=1)
     return tuple(
         (

time: 240 us -> 363 us (1.51)
  waiting for transfers between devices: 91.9 us -> 180 us
  blocking collectives: 68 us -> 101 us
  starting transfers between devices: 11.2 us -> 25.6 us
  between operations: 13.7 us -> 0.32 us
    all_to_all x0 -> x1, waiting for transfers between devices: none -> 162 us  [swapped_in(): shards = lax.all_to_all(shards, name, split_axis=0, concat_axis=0)]
    all_gather x1 -> x0, waiting for transfers between devices: 69.1 us -> none  [turned_gather(): filled = lax.all_gather(both, axis, axis=0, tiled=True)]
    all_gather x2, blocking collectives: 49.6 us -> 82.6 us  [collected_together(): both, at, found = (lax.all_gather(jnp.concatenate(lines), axis), 0, {})]
    all_to_all x0 -> x1, starting transfers between devices: none -> 16.1 us  [swapped_in(): shards = lax.all_to_all(shards, name, split_axis=0, concat_axis=0)]
    all_to_all x2, waiting for transfers between devices: 19.2 us -> 13.5 us  [from_everyone(): return lax.all_to_all(copies, axis, split_axis=0, concat_axis=0, tiled=True)]
where the time goes in v1:
time: 363 us; the launch traced here: 360 us
  waiting for transfers between devices  180 us (50%)
  blocking collectives  101 us (28%)
  local copies, waits for them, and re-layouts  33.3 us (9%)
  starting transfers between devices  25.6 us (7%)
  matrix products  13.2 us (4%)
  other arithmetic  6.73 us (2%)
    all_to_all x1, waiting for transfers between devices, swapped_in(): shards = lax.all_to_all(shards, name, split_axis=0, concat_axis=0)  162 us
    all_gather x2, blocking collectives, collected_together(): both, at, found = (lax.all_gather(jnp.concatenate(lines), axis), 0, {})  82.6 us
    dynamic_slice x31, local copies, waits for them, and re-layouts, add_tap(): taps = lax.dynamic_slice_in_dim(conv_kernel, tap_index, 1, 0)  21.9 us
    all_to_all x1, blocking collectives, sent_and_summed(): lax.all_to_all(pieces, axis, split_axis=0, concat_axis=0, tiled=True)  18.4 us
    all_to_all x1, starting transfers between devices, swapped_in(): shards = lax.all_to_all(shards, name, split_axis=0, concat_axis=0)  16.1 us
    all_to_all x2, waiting for transfers between devices, from_everyone(): return lax.all_to_all(copies, axis, split_axis=0, concat_axis=0, tiled=True)  13.5 us
    dot_general x5, matrix products, on_device(): jnp.dot(normed, weight, preferred_element_type=jnp.float32)  7.78 us
    all_to_all x2, starting transfers between devices, from_everyone(): return lax.all_to_all(copies, axis, split_axis=0, concat_axis=0, tiled=True)  7.64 us
  transfers between devices with their start and end apart: 4, of which 4 were waited for; matrix products, arithmetic and copies ran while one was open for 3% of the time, Pallas kernels for 0%

profile of v1, /device:TPU:64, one launch (start us, length us, event | category | flops | bytes accessed | tf_op | source)
XLA Modules:
  0.0 360.4 jit_solution(10920414817887679624)
XLA Ops:
  0.0 2.0 broadcast_in_dim.19
  2.0 4.3 %all-to-all-start = ((bf16[8,32,2048]{2,1,0:T(8,128)(2,1)}), bf16[8,32,2048]{2,1,0:T(8,128)(2,1)S(1)}, u32[]{:S(2)}, u32[]{:S(2)}) async-start(bf16[8,32,2048]{2,1,0:T(8,128)(2,1)} %broadcast_in_dim.19), calls=%async_computation | async-start | bytes 2097152 | tf_op jit(solution)/shard_map/all_to_all | solution.py:38
  9.1 0.7 constant_dynamic-update-slice_fusion.3
  12.0 10.3 %all-to-all-done = bf16[8,32,2048]{2,1,0:T(8,128)(2,1)S(1)} async-done(((bf16[8,32,2048]{2,1,0:T(8,128)(2,1)}), bf16[8,32,2048]{2,1,0:T(8,128)(2,1)S(1)}, u32[]{:S(2)}, u32[]{:S(2)}) %all-to-all-start) | async-done | bytes 1048608 | tf_op jit(solution)/shard_map/all_to_all | solution.py:38
  22.2 3.0 stack.2
  25.2 16.1 %all-to-all-start.1 = ((bf16[64,32,1408]{2,1,0:T(8,128)(2,1)}), bf16[64,32,1408]{2,1,0:T(8,128)(2,1)}, u32[]{:S(2)}, u32[]{:S(2)}) async-start(bf16[64,32,1408]{2,1,0:T(8,128)(2,1)} %stack.2), calls=%async_computation.1 | async-start | bytes 11534336 | tf_op jit(solution)/shard_map/all_to_all | solution.py:18
  42.1 161.7 %all-to-all-done.1 = bf16[64,32,1408]{2,1,0:T(8,128)(2,1)} async-done(((bf16[64,32,1408]{2,1,0:T(8,128)(2,1)}), bf16[64,32,1408]{2,1,0:T(8,128)(2,1)}, u32[]{:S(2)}, u32[]{:S(2)}) %all-to-all-start.1) | async-done | bytes 5767200 | tf_op jit(solution)/shard_map/all_to_all | solution.py:18
  203.8 1.5 convolution_convert_fusion.5
  205.3 1.5 divide_multiply_fusion
  206.8 1.7 fusion.17
  208.5 1.5 log-plus-one_add_fusion
  210.3 1.5 while.31
  211.9 45.3 %all-gather.2 = bf16[8,129,128]{2,1,0:T(8,128)(2,1)S(1)} all-gather(bf16[1,129,128]{2,1,0:T(8,128)(2,1)S(1)} %maximum_bitcast_fusion), channel_id=2, replica_groups=mesh['sp_0'=8,'sp_1'=8,'tp'=8] {'sp_1'}, dimensions={0}, use_global_device_ids=true | all-gather | bytes 297216 | tf_op jit(solution)/shard_map/all_gather | solution.py:66
  257.5 37.3 %all-gather.3 = bf16[8,129,128]{2,1,0:T(8,128)(2,1)S(1)} all-gather(bf16[1,129,128]{2,1,0:T(8,128)(2,1)S(1)} %maximum_bitcast_fusion.1), channel_id=3, replica_groups=mesh['sp_0'=8,'sp_1'=8,'tp'=8] {'sp_0'}, dimensions={0}, use_global_device_ids=true | all-gather | bytes 297216 | tf_op jit(solution)/shard_map/all_gather | solution.py:66
  294.7 1.7 fusion.16
  296.5 1.9 collective-permute-start
  299.9 4.3 %collective-permute-done = bf16[30,256]{1,0:T(8,128)(2,1)S(1)} collective-permute-done((bf16[30,256]{1,0:T(8,128)(2,1)S(1)}, bf16[30,256]{1,0:T(8,128)(2,1)S(1)}, u32[]{:S(2)}, u32[]{:S(2)}) %collective-permute-start) | collective-permute-done | bytes 15392 | tf_op jit(solution)/shard_map/ppermute | solution.py:100
  304.2 25.7 %while.32 = (s32[]{:T(128)}, f32[256,256]{1,0:T(8,128)S(1)}, f32[31,256]{1,0:T(8,128)}, f32[286,256]{1,0:T(8,128)S(1)}, s32[]{:T(128)}, /*index=5*/s32[]{:T(128)}) while((s32[]{:T(128)}, f32[256,256]{1,0:T(8,128)S(1)}, f32[31,256]{1,0:T(8,128)}, f32[286,256]{1,0:T(8,128)S(1)}, s32[]{:T(128)}, /*index=5*/s32[]{:T(128)}) %tuple.82), condition=%wide.region_6.7_spmd.clone, body=%wide.region_5.6_spmd.clone.sunk | while | flops 196611 | bytes 789599 | solution.py:266
  330.7 3.3 all-to-all-start.2
  334.1 2.0 fusion.30
  336.1 3.3 all-to-all-done.2
  339.4 1.8 fusion.7
  341.2 18.4 %all_to_all.21 = bf16[8,32,2048]{2,1,0:T(8,128)(2,1)S(1)} all-to-all(bf16[8,32,2048]{2,1,0:T(8,128)(2,1)S(1)} %bitcast.159), channel_id=1, replica_groups=mesh['sp_0'=8,'sp_1'=8,'tp'=8] {'tp'}, dimensions={0} | all-to-all | bytes 2097152 | tf_op jit(solution)/shard_map/all_to_all | solution.py:123
  359.6 0.8 reduce_sum.62
  (126 shorter events, 35.2 us)
Async XLA Ops:
  2.0 20.2 %all-to-all-start = ((bf16[8,32,2048]{2,1,0:T(8,128)(2,1)}), bf16[8,32,2048]{2,1,0:T(8,128)(2,1)S(1)}, u32[]{:S(2)}, u32[]{:S(2)}) async-start(bf16[8,32,2048]{2,1,0:T(8,128)(2,1)} %broadcast_in_dim.19), calls=%async_computation | async-start | bytes 2097152 | tf_op jit(solution)/shard_map/all_to_all | solution.py:38
  25.2 16.6 %copy-start = (f32[2048]{0:T(1024)S(1)}, f32[2048]{0:T(1024)}, u32[]{:S(2)}) copy-start(f32[2048]{0:T(1024)} %param.21) | copy-start | bytes 24580
  25.2 178.6 %all-to-all-start.1 = ((bf16[64,32,1408]{2,1,0:T(8,128)(2,1)}), bf16[64,32,1408]{2,1,0:T(8,128)(2,1)}, u32[]{:S(2)}, u32[]{:S(2)}) async-start(bf16[64,32,1408]{2,1,0:T(8,128)(2,1)} %stack.2), calls=%async_computation.1 | async-start | bytes 11534336 | tf_op jit(solution)/shard_map/all_to_all | solution.py:18
  41.3 167.1 %copy-start.1 = (f32[256,128]{1,0:T(8,128)S(1)}, f32[256,128]{1,0:T(8,128)}, u32[]{:S(2)}) copy-start(f32[256,128]{1,0:T(8,128)} %param.27) | copy-start | bytes 393220
  41.3 167.1 %copy-start.2 = (f32[128]{0:T(128)S(1)}, f32[128]{0:T(128)}, u32[]{:S(2)}) copy-start(f32[128]{0:T(128)} %param.26) | copy-start | bytes 1540
  296.5 7.7 %collective-permute-start = (bf16[30,256]{1,0:T(8,128)(2,1)S(1)}, bf16[30,256]{1,0:T(8,128)(2,1)S(1)}, u32[]{:S(2)}, u32[]{:S(2)}) collective-permute-start(bf16[30,256]{1,0:T(8,128)(2,1)S(1)} %slice.229), channel_id=1, source_target_pairs={{0,8},{8,16},{16,24},{24,32},{32,40},{40,48},{48,56},{56,64},{64,7... | collective-permute-start | bytes 46088 | tf_op jit(solution)/shard_map/ppermute | solution.py:100
  330.7 8.6 %all-to-all-start.2 = ((f32[8,1,512]{2,1,0:T(1,128)}), f32[8,1,512]{2,1,0:T(1,128)S(1)}, u32[]{:S(2)}, u32[]{:S(2)}) async-start(f32[8,1,512]{2,1,0:T(1,128)} %broadcast_in_dim.23), calls=%async_computation.2 | async-start | bytes 32768 | tf_op jit(solution)/shard_map/all_to_all | solution.py:38
